TPU v7x, 512 devices: a whole 4x4x16 slice. The times are simulated.
512 devices in a mesh: sp: 16 (over z), fs: 4 (over y), tp: 8 (over x, core).
Axes of the slice: x: 4, y: 4, z: 16, core: 2. Of those that a mesh axis runs over, the one named last changes fastest.
Arguments:
- inputs: bfloat16 [4, 4096, 4096], P('fs', 'sp', 'tp'), may hold values from -6 to 6
- norm_gain: float32 [4096], replicated, may hold values from 0.1 to 1.9
- conv_in_a: bfloat16 [4096, 1024], P(('sp', 'fs'), 'tp'), may hold values from -0.09375 to 0.09375
- conv_in_b: bfloat16 [4096, 1024], P(('sp', 'fs'), 'tp'), may hold values from -0.09375 to 0.09375
- query_w: bfloat16 [4096, 512], P(('sp', 'fs'), 'tp'), may hold values from -0.09375 to 0.09375
- key_w: bfloat16 [4096, 512], P(('sp', 'fs'), 'tp'), may hold values from -0.09375 to 0.09375
- value_w: bfloat16 [4096, 1024], P(('sp', 'fs'), 'tp'), may hold values from -0.09375 to 0.09375
- out_gate_w: bfloat16 [4096, 1024], P(('sp', 'fs'), 'tp'), may hold values from -0.09375 to 0.09375
- pointwise_w: bfloat16 [4096, 1024], P(('sp', 'fs'), 'tp'), may hold values from -0.1875 to 0.1875
- gla_out_w: bfloat16 [4096, 1024], P(('sp', 'fs'), 'tp'), may hold values from -0.1875 to 0.1875
- forget_first_factor: bfloat16 [4096, 64], replicated, may hold values from -0.09375 to 0.09375
- decay_w: bfloat16 [64, 512], replicated, may hold values from -0.75 to 0.75
- decay_bias: float32 [512], replicated, as said below
- decay_extra: float32 [4, 4096, 512], P('fs', 'sp', 'tp'), may hold values from -2.2 to 0, as said below
- conv_kernel: float32 [31, 1024], replicated, may hold values from -7 to 7
- conv_gain: float32 [1024], replicated, may hold values from 0.1 to 1.9
- head_gain: float32 [64], replicated, may hold values from 0.1 to 1.9
Outputs:
- mixed: bfloat16 [4, 4096, 4096], P('fs', 'sp', 'tp')
Inputs may be any that keep to these rules, and one draw needn't show every extreme that they name: decay_bias is positive. decay_extra is never positive.
All inputs are finite; a program needn't handle non-finite values.
Results may differ from a plain program's by a relative error of at most 0.015.
Values may be sent and summed in bfloat16 or wider, within the bound.
A program may use at most 128 MiB of HBM per device.

v0:
```python
import jax
import jax.numpy as jnp
from jax import lax
from jax.sharding import PartitionSpec as P

DK = 32
DV = 64
BLOCK = 64


def side_by_side(arrays, axis, dim, along):
    ends, at = ([], 0)
    for a in arrays[:-1]:
        at += a.shape[along]
        ends.append(at)
    both = jnp.concatenate(arrays, axis=along)
    return tuple(jnp.split(lax.all_gather(both, axis, axis=dim, tiled=True), ends, axis=along))


def from_everyone(value, axis):
    length = lax.axis_size(axis)
    return lax.all_to_all(
        jnp.broadcast_to(value[None], (length, *value.shape)), axis, 0, 0, tiled=True
    )


def in_order(tiles, dim):
    lengths = list(tiles.shape[1:])
    lengths[dim] *= tiles.shape[0]
    return jnp.moveaxis(tiles, 0, dim).reshape(lengths)


def gathered_copies(value, axis, dim):
    tiles = from_everyone(value, axis)
    return in_order(tiles, dim)


def from_behind(value, axis, by):
    length = lax.axis_size(axis)
    pairs = [(i, i + by) for i in range(length) if 0 <= i + by < length]
    return lax.ppermute(value, axis, pairs)


def over_copies(value, axis):
    everything = from_everyone(value, axis)
    return jnp.sum(everything, axis=0)


def in_one(arrays, axis):
    vector, at, outs = (jnp.concatenate([a.reshape(-1) for a in arrays]), 0, [])
    subtotal = over_copies(vector, axis)
    for a in arrays:
        outs.append(subtotal[at : at + a.size].reshape(a.shape))
        at += a.size
    return tuple(outs)


def in_blocks(value, dim, length):
    lengths = value.shape
    tiles = value.reshape(*lengths[:dim], length, lengths[dim] // length, *lengths[dim + 1 :])
    return jnp.moveaxis(tiles, dim, 0)


def sum_at_owner(value, axis, dim):
    length = lax.axis_size(axis)
    tiles = lax.all_to_all(in_blocks(value, dim, length), axis, 0, 0, tiled=True)
    return jnp.sum(tiles.astype(jnp.float32), axis=0)


def shards(
    inputs,
    norm_gain,
    conv_in_a,
    conv_in_b,
    query_w,
    key_w,
    value_w,
    out_gate_w,
    pointwise_w,
    gla_out_w,
    forget_first_factor,
    decay_w,
    decay_bias,
    decay_extra,
    conv_kernel,
    conv_gain,
    head_gain,
):
    nearer = side_by_side(
        (conv_in_a, conv_in_b, query_w, key_w, value_w, out_gate_w, pointwise_w, gla_out_w),
        "fs",
        0,
        1,
    )
    collected = side_by_side(
        (nearer[0], nearer[1], nearer[2], nearer[3], nearer[4], nearer[5], nearer[6], nearer[7]),
        "sp",
        0,
        1,
    )
    (
        conv_a_full,
        conv_b_full,
        query_full,
        key_full,
        value_full,
        gate_full,
        pointwise_full,
        gla_out_full,
    ) = collected
    tok_rows = inputs[0]
    token_count = tok_rows.shape[0]
    in_weights = (
        conv_a_full,
        conv_b_full,
        query_full,
        key_full,
        value_full,
        gate_full,
        forget_first_factor,
    )
    segment_values = gathered_copies(tok_rows, "tp", 1).astype(jnp.float32)
    scaled = (segment_values * norm_gain).astype(jnp.bfloat16)
    sums = tuple(
        (jnp.dot(scaled, weight, preferred_element_type=jnp.float32) for weight in in_weights)
    )
    sums, squares = (sums, jnp.sum(segment_values * segment_values, axis=1))
    row_scale = lax.rsqrt(squares / norm_gain.shape[0] + 1e-06)[:, None]
    conv_a, conv_b, queries, keys, values, out_gate, low_rank = [
        (running * row_scale).astype(jnp.bfloat16) for running in sums
    ]
    gated = (conv_a.astype(jnp.float32) * jax.nn.sigmoid(conv_b.astype(jnp.float32))).astype(
        jnp.bfloat16
    )
    reach = conv_kernel.shape[0] - 1
    earlier = from_behind(gated[token_count - reach :], "sp", 1)
    extended = jnp.concatenate([earlier, gated], axis=0).astype(jnp.float32)
    tp_index = lax.axis_index("tp")
    channels = gated.shape[1]
    kernel = lax.dynamic_slice_in_dim(conv_kernel, tp_index * channels, channels, 1)
    convolved = jnp.zeros((token_count, channels), jnp.float32)
    for offset in range(reach + 1):
        convolved = convolved + kernel[offset] * extended[offset : offset + token_count]
    channel_sum, channel_squares = in_one(
        (jnp.sum(convolved, axis=1), jnp.sum(convolved * convolved, axis=1)), "tp"
    )
    total_channels = conv_gain.shape[0]
    average = channel_sum / total_channels
    spread_squared_mean = channel_squares / total_channels - average * average
    gain_part = lax.dynamic_slice_in_dim(conv_gain, tp_index * channels, channels)
    normed = (
        (convolved - average[:, None]) * lax.rsqrt(spread_squared_mean + 1e-05)[:, None] * gain_part
    )
    conv_act = jax.nn.silu(normed).astype(jnp.bfloat16)
    key_width = keys.shape[1]
    head_count = key_width // DK
    decay_part = lax.dynamic_slice_in_dim(decay_w, tp_index * key_width, key_width, 1)
    bias_part = lax.dynamic_slice_in_dim(decay_bias, tp_index * key_width, key_width)
    pre_decay = jnp.dot(low_rank, decay_part, preferred_element_type=jnp.float32) + bias_part
    log_decay = jax.nn.log_sigmoid(pre_decay) / 16.0 + decay_extra[0]
    block_count = token_count // BLOCK
    highest = lax.Precision.HIGHEST

    def split_blocks(array_operand, width):
        return array_operand.reshape(block_count, BLOCK, head_count, width).transpose(0, 2, 1, 3)

    q_blocks = split_blocks(queries.astype(jnp.float32), DK) * DK ** (-0.5)
    k_blocks = split_blocks(keys.astype(jnp.float32), DK)
    v_blocks = split_blocks(values.astype(jnp.float32), DV)
    prefix_running_sum = jnp.cumsum(split_blocks(log_decay, DK), axis=2)
    causal = jnp.tril(jnp.ones((BLOCK, BLOCK), dtype=bool))
    spread = prefix_running_sum[:, :, :, None, :] - prefix_running_sum[:, :, None, :, :]
    weights_in = jnp.exp(jnp.where(causal[:, :, None], spread, -jnp.inf))
    scores = jnp.einsum("nhid,nhjd,nhijd->nhij", q_blocks, k_blocks, weights_in, precision=highest)
    inner = jnp.einsum("nhij,nhjv->nhiv", scores, v_blocks, precision=highest)
    block_total = prefix_running_sum[:, :, -1]
    block_state = jnp.einsum(
        "nhjd,nhjv->nhdv",
        k_blocks * jnp.exp(block_total[:, :, None] - prefix_running_sum),
        v_blocks,
        precision=highest,
    )

    def advance(state, block_pair):
        decay_row, added_share_term = block_pair
        return (jnp.exp(decay_row)[..., None] * state + added_share_term, state)

    local_final, local_entering = lax.scan(
        advance, jnp.zeros((head_count, DK, DV), jnp.float32), (block_total, block_state)
    )
    device_total = jnp.sum(block_total, axis=0)
    totals = lax.all_gather(device_total[None], "sp", axis=0, tiled=True)
    running_totals = jnp.cumsum(totals, axis=0)
    sp_index = lax.axis_index("sp")
    before = lax.dynamic_index_in_dim(
        running_totals, sp_index, 0, False
    ) - lax.dynamic_index_in_dim(totals, sp_index, 0, False)
    piece = lax.all_gather(local_final[None], "sp", axis=0, tiled=True)
    number = piece.shape[0]
    anchor = jnp.arange(number, dtype=jnp.int32)
    exponent = jnp.where(
        (anchor < sp_index)[:, None, None], before[None] - running_totals, -jnp.inf
    )
    entering = jnp.einsum("nhd,nhdv->hdv", jnp.exp(exponent), piece, precision=highest)
    passed = jnp.exp(jnp.cumsum(block_total, axis=0) - block_total)
    entering_blocks = passed[..., None] * entering[None] + local_entering
    outer = jnp.einsum(
        "nhid,nhdv->nhiv",
        q_blocks * jnp.exp(prefix_running_sum),
        entering_blocks,
        precision=highest,
    )
    head_output = inner + outer
    normed_heads = (
        head_output
        * lax.rsqrt(jnp.mean(head_output * head_output, axis=-1, keepdims=True) + 1e-06)
        * head_gain
    )
    gla_rows = normed_heads.transpose(0, 2, 1, 3).reshape(token_count, head_count * DV)
    gla_act = (gla_rows * jax.nn.silu(out_gate.astype(jnp.float32))).astype(jnp.bfloat16)
    contract = (((1,), (1,)), ((), ()))
    conv_term = lax.dot_general(
        pointwise_full, conv_act, contract, preferred_element_type=jnp.float32
    )
    summed = sum_at_owner(
        (
            conv_term
            + lax.dot_general(gla_out_full, gla_act, contract, preferred_element_type=jnp.float32)
        ).astype(jnp.bfloat16),
        "tp",
        0,
    )
    return (tok_rows.astype(jnp.float32) + summed.T).astype(jnp.bfloat16)[None]


def solution(mesh):
    return jax.shard_map(
        shards,
        mesh=mesh,
        in_specs=(
            P("fs", "sp", "tp"),
            P(),
            P(("sp", "fs"), "tp"),
            P(("sp", "fs"), "tp"),
            P(("sp", "fs"), "tp"),
            P(("sp", "fs"), "tp"),
            P(("sp", "fs"), "tp"),
            P(("sp", "fs"), "tp"),
            P(("sp", "fs"), "tp"),
            P(("sp", "fs"), "tp"),
            P(),
            P(),
            P(),
            P("fs", "sp", "tp"),
            P(),
            P(),
            P(),
        ),
        out_specs=P("fs", "sp", "tp"),
        check_vma=False,
    )
```

profile of v0, /device:TPU:1, one launch (start us, length us, event | category | flops | bytes accessed | tf_op | source)
XLA Modules:
  0.0 245.8 jit_solution(409942196637541957)
XLA Ops:
  6.5 1.0 concatenate.11
  7.5 12.3 %all_gather.12 = bf16[256,896]{1,0:T(8,128)(2,1)} all-gather(bf16[64,896]{1,0:T(8,128)(2,1)S(1)} %concatenate.11), channel_id=1, replica_groups=mesh['sp'=16,'fs'=4,'tp'=8] {'fs'}, dimensions={0}, use_global_device_ids=true | all-gather | bytes 573440 | tf_op jit(solution)/shard_map/all_gather | solution.py:17
  19.8 0.0 all-gather.5.cloned.1.call-update
  19.8 1.1 copy.64
  20.9 1.5 broadcast_in_dim.45
  22.4 11.6 %all-to-all-start = ((bf16[8,256,512]{1,2,0:T(8,128)(2,1)}), bf16[8,256,512]{1,2,0:T(8,128)(2,1)S(1)}, u32[]{:S(2)}, u32[]{:S(2)}) async-start(bf16[8,256,512]{1,2,0:T(8,128)(2,1)} %broadcast_in_dim.45), calls=%async_computation | async-start | bytes 4194304 | tf_op jit(solution)/shard_map/all_to_all | solution.py:22
  34.0 0.8 dynamic_slice.30
  34.8 1.3 dynamic_slice.28
  36.1 1.7 dynamic-slice_bitcast_fusion.29
  37.8 1.9 fusion.98
  39.7 20.6 %all-to-all-done = bf16[8,256,512]{1,2,0:T(8,128)(2,1)S(1)} async-done(((bf16[8,256,512]{1,2,0:T(8,128)(2,1)}), bf16[8,256,512]{1,2,0:T(8,128)(2,1)S(1)}, u32[]{:S(2)}, u32[]{:S(2)}) %all-to-all-start) | async-done | bytes 2097184 | tf_op jit(solution)/shard_map/all_to_all | solution.py:22
  60.3 0.6 multiply_reduce_fusion
  60.9 1.8 fusion.2
  62.6 2.2 fusion.86
  64.9 0.1 reshape.75
  65.0 0.1 copy.66
  65.1 0.2 reduce_window_sum.35
  65.4 0.1 copy.67
  65.5 28.2 %all-gather.2 = f32[16,2,32]{2,1,0:T(2,128)S(1)} all-gather(f32[1,2,32]{2,1,0:T(2,128)S(1)} %bitcast.160), channel_id=2, replica_groups=mesh['sp'=16,'fs'=4,'tp'=8] {'sp'}, dimensions={0}, use_global_device_ids=true | all-gather | bytes 4352 | tf_op jit(solution)/shard_map/all_gather | solution.py:192
  93.8 0.1 exponential_bitcast_fusion.1
  93.9 0.1 copy.87
  94.0 4.6 %select_exponential_fusion = f32[4,2,64,64,32]{3,4,2,1,0:T(8,128)} fusion(f32[4,2,64,32]{2,3,1,0:T(8,128)S(1)} %copy.67, f32[4,2,64,32]{3,2,1,0:T(8,128)S(1)} %reduce_window_sum.35, pred[64,64]{1,0:T(8,128)(4,1)S(1)} %iota_compare_fusion), kind=kLoop, calls=%fused_computation.5 | loop fusion | flops 2097152 | bytes 4329472 | tf_op jit(solution)/shard_map/exp | solution.py:173
  98.5 11.0 %copy.82 = f32[4,2,64,64,32]{2,3,4,1,0:T(8,128)} copy(f32[4,2,64,64,32]{3,4,2,1,0:T(8,128)} %select_exponential_fusion) | data formatting | bytes 8388608
  109.6 12.5 %all-gather.5.cloned.1.call-done = bf16[4096,896]{1,0:T(8,128)(2,1)} async-done(((bf16[256,896]{1,0:T(8,128)(2,1)}), bf16[4096,896]{1,0:T(8,128)(2,1)}) %all-gather.5.cloned.1.call-update) | async-done | bytes 7340048 | tf_op jit(solution)/shard_map/all_gather | solution.py:17
  122.1 2.2 fusion.18
  124.3 0.1 reshape.81
  124.4 0.8 copy.73
  125.3 2.0 fusion.13
  127.3 0.1 reshape.77
  127.4 2.0 fusion.38
  129.4 5.8 %while.13 = (s32[]{:T(128)}, f32[2,32,64]{2,1,0:T(8,128)S(1)}, f32[4,2,32,64]{3,2,1,0:T(8,128)}, f32[4,2,32]{2,1,0:T(2,128)S(1)}, f32[4,2,32,64]{3,2,1,0:T(8,128)}, /*index=5*/s32[]{:T(128)}, s32[]{:T(128)}) while((s32[]{:T(128)}, f32[2,32,64]{2,1,0:T(8,128)S(1)}, f32[4,2,32,64]{3,2,1,0:T(8,128)}, f32[4,2,32]{2,1,0:T(2,128)S(1)}, ...), condition=%wide.region_9.10_spmd.clone, body=%wide.region_8.9_spmd.clone.sunk | while | flops 16387 | bytes 99680 | solution.py:188
  129.4 0.6 bitcast_dynamic-update-slice_fusion.2
  130.0 0.8 bitcast_add_fusion.3
  130.8 0.6 bitcast_dynamic-update-slice_fusion.2
  131.4 0.8 bitcast_add_fusion.3
  132.3 0.6 bitcast_dynamic-update-slice_fusion.2
  132.9 0.8 bitcast_add_fusion.3
  133.7 0.6 bitcast_dynamic-update-slice_fusion.2
  134.3 0.8 bitcast_add_fusion.3
  135.2 25.9 %all-gather.1 = f32[32,32,64]{2,1,0:T(8,128)} all-gather(f32[2,32,64]{2,1,0:T(8,128)S(1)} %get-tuple-element.33), channel_id=3, replica_groups=mesh['sp'=16,'fs'=4,'tp'=8] {'sp'}, dimensions={0}, use_global_device_ids=true | all-gather | bytes 278528 | tf_op jit(solution)/shard_map/all_gather | solution.py:198
  161.1 0.7 copy.68
  161.7 1.8 fusion.21
  163.5 0.1 mul.589
  163.6 0.8 copy.72
  164.5 5.3 %fusion = f32[4,2,64,64]{2,3,1,0:T(8,128)S(1)} fusion(f32[4,2,64,64,32]{2,3,4,1,0:T(8,128)} %copy.82, f32[4,2,32,64]{3,2,1,0:T(8,128)S(1)} %copy.69, f32[4,2,32,64]{3,2,1,0:T(8,128)} %copy.68), kind=kLoop, calls=%fused_computation.4 | loop fusion | flops 3112960 | bytes 4456448 | tf_op jit(solution)/shard_map/nhid,nhjd,nhijd->nhij/dot_general | solution.py:174
  169.8 0.3 fusion.73
  170.4 2.0 fusion.12
  172.4 2.0 fusion.6
  174.4 2.2 collective-permute-start
  176.7 0.9 fusion.34
  177.6 0.8 multiply_reduce_fusion.1
  178.7 1.2 fusion.101
  179.8 0.6 broadcast_in_dim.46
  180.4 12.4 %all-to-all-start.1 = ((f32[8,1,512]{2,1,0:T(1,128)}), f32[8,1,512]{2,1,0:T(1,128)S(1)}, u32[]{:S(2)}, u32[]{:S(2)}) async-start(f32[8,1,512]{2,1,0:T(1,128)} %broadcast_in_dim.46), calls=%async_computation.1 | async-start | bytes 32768 | tf_op jit(solution)/shard_map/all_to_all | solution.py:22
  192.9 0.7 fusion.37
  193.6 0.2 copy.76
  193.8 0.2 reshape.78
  194.0 3.6 %all-to-all-done.1 = f32[8,1,512]{2,1,0:T(1,128)S(1)} async-done(((f32[8,1,512]{2,1,0:T(1,128)}), f32[8,1,512]{2,1,0:T(1,128)S(1)}, u32[]{:S(2)}, u32[]{:S(2)}) %all-to-all-start.1) | async-done | bytes 16416 | tf_op jit(solution)/shard_map/all_to_all | solution.py:22
  197.6 4.1 %fusion.31 = f32[4096,256]{1,0:T(8,128)} fusion(bf16[4096,896]{1,0:T(8,128)(2,1)} %all-gather.5.cloned.1.call-done, f32[256,128]{1,0:T(8,128)} %get-tuple-element.65, f32[128]{0:T(128)} %dynamic_slice.28, f32[256]{0:T(256)S(1)} %get-tuple-element.100, f32[256]{0:T(256)S(1)} %get-tuple-element.99), kind=kOutput, calls=%fused_computation.50 | convolution fusion | flops 268697600 | bytes 5376512 | tf_op jit(solution)/shard_map/dot_general | solution.py:222
  201.7 5.7 %fusion.1 = bf16[4096,256]{1,0:T(8,128)(2,1)} fusion(f32[4096,256]{1,0:T(8,128)} %fusion.31, bf16[4096,896]{1,0:T(8,128)(2,1)} %all-gather.5.cloned.1.call-done, f32[256,128]{1,0:T(8,128)S(1)} %reshape.78, bf16[256,4096]{0,1:T(8,128)(2,1)S(1)} %copy-done.1, f32[256]{0:T(256)S(1)} %add_rsqrt_fusion.1), kind=kOutput, calls=%fused_computation.7 | convolution fusion | flops 539262976 | bytes 10617856 | tf_op jit(solution)/shard_map/dot_general | solution.py:228
  207.3 30.4 %all_to_all.16 = bf16[8,512,256]{2,1,0:T(8,128)(2,1)S(1)} all-to-all(bf16[8,512,256]{2,1,0:T(8,128)(2,1)} %bitcast.150), channel_id=1, replica_groups=mesh['sp'=16,'fs'=4,'tp'=8] {'tp'}, dimensions={0} | all-to-all | bytes 4194304 | tf_op jit(solution)/shard_map/all_to_all | solution.py:66
  237.7 0.3 convert_reduce_fusion
  238.0 0.1 fusion.36
  238.1 0.8 copy.77
  (96 shorter events, 0.4 us)
Async XLA Ops:
  6.5 56.1 %copy-start = (bf16[4096,64]{0,1:T(8,128)(2,1)S(1)}, bf16[4096,64]{0,1:T(8,128)(2,1)}, u32[]{:S(2)}) copy-start(bf16[4096,64]{0,1:T(8,128)(2,1)} %param.29) | copy-start | bytes 1572868
  6.5 115.5 %all-gather.5.cloned.1.call-start = ((), (), s32[]{:S(2)}) async-start(), calls=%async_computation.3 | async-start | bytes 7798784 | tf_op jit(solution)/shard_map/all_gather | solution.py:17
  20.9 39.9 %copy-start.6 = (f32[4096]{0:T(1024)S(1)}, f32[4096]{0:T(1024)}, u32[]{:S(2)}) copy-start(f32[4096]{0:T(1024)} %param.20) | copy-start | bytes 49156
  22.4 37.8 %all-to-all-start = ((bf16[8,256,512]{1,2,0:T(8,128)(2,1)}), bf16[8,256,512]{1,2,0:T(8,128)(2,1)S(1)}, u32[]{:S(2)}, u32[]{:S(2)}) async-start(bf16[8,256,512]{1,2,0:T(8,128)(2,1)} %broadcast_in_dim.45), calls=%async_computation | async-start | bytes 4194304 | tf_op jit(solution)/shard_map/all_to_all | solution.py:22
  34.0 28.6 %copy-start.5 = (f32[1,256,64]{1,2,0:T(8,128)S(1)}, f32[1,256,64]{1,2,0:T(8,128)}, u32[]{:S(2)}) copy-start(f32[1,256,64]{1,2,0:T(8,128)} %param.32) | copy-start | bytes 196612
  98.5 23.5 %copy-start.1 = (bf16[256,4096]{0,1:T(8,128)(2,1)S(1)}, bf16[256,4096]{0,1:T(8,128)(2,1)}, u32[]{:S(2)}) copy-start(bf16[256,4096]{0,1:T(8,128)(2,1)} %fusion.2) | copy-start | bytes 6291460
  169.8 6.9 %copy-start.2 = (f32[32,32,64]{2,1,0:T(8,128)S(1)}, f32[32,32,64]{2,1,0:T(8,128)}, u32[]{:S(2)}) copy-start(f32[32,32,64]{2,1,0:T(8,128)} %all-gather.1) | copy-start | bytes 786436
  170.1 7.4 %copy-start.3 = (f32[4,64,2,32]{3,1,2,0:T(8,128)S(1)}, f32[4,64,2,32]{3,1,2,0:T(8,128)}, u32[]{:S(2)}) copy-start(f32[4,64,2,32]{3,1,2,0:T(8,128)} %copy.72) | copy-start | bytes 196612
  170.1 7.4 %copy-start.4 = (f32[4,2,32,64]{3,2,1,0:T(8,128)S(1)}, f32[4,2,32,64]{3,2,1,0:T(8,128)}, u32[]{:S(2)}) copy-start(f32[4,2,32,64]{3,2,1,0:T(8,128)} %get-tuple-element.34) | copy-start | bytes 196612
  170.1 8.2 %copy-start.7 = (f32[128]{0:T(128)S(1)}, f32[128]{0:T(128)}, u32[]{:S(2)}) copy-start(f32[128]{0:T(128)} %get-tuple-element.69) | copy-start | bytes 1540
  170.1 8.2 %copy-start.8 = (f32[128]{0:T(128)S(1)}, f32[128]{0:T(128)}, u32[]{:S(2)}) copy-start(f32[128]{0:T(128)} %get-tuple-element.70) | copy-start | bytes 1540
  170.1 8.2 %copy-start.9 = (f32[128]{0:T(128)S(1)}, f32[128]{0:T(128)}, u32[]{:S(2)}) copy-start(f32[128]{0:T(128)} %get-tuple-element.71) | copy-start | bytes 1540
  170.2 8.2 %copy-start.10 = (f32[128]{0:T(128)S(1)}, f32[128]{0:T(128)}, u32[]{:S(2)}) copy-start(f32[128]{0:T(128)} %get-tuple-element.72) | copy-start | bytes 1540
  170.2 8.2 %copy-start.11 = (f32[128]{0:T(128)S(1)}, f32[128]{0:T(128)}, u32[]{:S(2)}) copy-start(f32[128]{0:T(128)} %get-tuple-element.73) | copy-start | bytes 1540
  170.2 8.2 %copy-start.12 = (f32[128]{0:T(128)S(1)}, f32[128]{0:T(128)}, u32[]{:S(2)}) copy-start(f32[128]{0:T(128)} %get-tuple-element.74) | copy-start | bytes 1540
  170.2 8.2 %copy-start.13 = (f32[128]{0:T(128)S(1)}, f32[128]{0:T(128)}, u32[]{:S(2)}) copy-start(f32[128]{0:T(128)} %get-tuple-element.75) | copy-start | bytes 1540
  170.2 8.2 %copy-start.14 = (f32[128]{0:T(128)S(1)}, f32[128]{0:T(128)}, u32[]{:S(2)}) copy-start(f32[128]{0:T(128)} %get-tuple-element.76) | copy-start | bytes 1540
  170.2 8.2 %copy-start.15 = (f32[128]{0:T(128)S(1)}, f32[128]{0:T(128)}, u32[]{:S(2)}) copy-start(f32[128]{0:T(128)} %get-tuple-element.77) | copy-start | bytes 1540
  170.2 8.2 %copy-start.16 = (f32[128]{0:T(128)S(1)}, f32[128]{0:T(128)}, u32[]{:S(2)}) copy-start(f32[128]{0:T(128)} %get-tuple-element.78) | copy-start | bytes 1540
  170.2 8.2 %copy-start.17 = (f32[128]{0:T(128)S(1)}, f32[128]{0:T(128)}, u32[]{:S(2)}) copy-start(f32[128]{0:T(128)} %get-tuple-element.79) | copy-start | bytes 1540
  170.2 8.2 %copy-start.18 = (f32[128]{0:T(128)S(1)}, f32[128]{0:T(128)}, u32[]{:S(2)}) copy-start(f32[128]{0:T(128)} %get-tuple-element.80) | copy-start | bytes 1540
  170.2 8.2 %copy-start.19 = (f32[128]{0:T(128)S(1)}, f32[128]{0:T(128)}, u32[]{:S(2)}) copy-start(f32[128]{0:T(128)} %get-tuple-element.81) | copy-start | bytes 1540
  170.3 8.2 %copy-start.20 = (f32[128]{0:T(128)S(1)}, f32[128]{0:T(128)}, u32[]{:S(2)}) copy-start(f32[128]{0:T(128)} %get-tuple-element.82) | copy-start | bytes 1540
  170.3 8.2 %copy-start.21 = (f32[128]{0:T(128)S(1)}, f32[128]{0:T(128)}, u32[]{:S(2)}) copy-start(f32[128]{0:T(128)} %get-tuple-element.83) | copy-start | bytes 1540
  170.3 8.2 %copy-start.22 = (f32[128]{0:T(128)S(1)}, f32[128]{0:T(128)}, u32[]{:S(2)}) copy-start(f32[128]{0:T(128)} %get-tuple-element.84) | copy-start | bytes 1540
  170.3 8.2 %copy-start.23 = (f32[128]{0:T(128)S(1)}, f32[128]{0:T(128)}, u32[]{:S(2)}) copy-start(f32[128]{0:T(128)} %get-tuple-element.85) | copy-start | bytes 1540
  170.3 8.2 %copy-start.24 = (f32[128]{0:T(128)S(1)}, f32[128]{0:T(128)}, u32[]{:S(2)}) copy-start(f32[128]{0:T(128)} %get-tuple-element.86) | copy-start | bytes 1540
  170.3 8.2 %copy-start.25 = (f32[128]{0:T(128)S(1)}, f32[128]{0:T(128)}, u32[]{:S(2)}) copy-start(f32[128]{0:T(128)} %get-tuple-element.87) | copy-start | bytes 1540
  170.3 8.2 %copy-start.26 = (f32[128]{0:T(128)S(1)}, f32[128]{0:T(128)}, u32[]{:S(2)}) copy-start(f32[128]{0:T(128)} %get-tuple-element.88) | copy-start | bytes 1540
  170.3 8.2 %copy-start.27 = (f32[128]{0:T(128)S(1)}, f32[128]{0:T(128)}, u32[]{:S(2)}) copy-start(f32[128]{0:T(128)} %get-tuple-element.89) | copy-start | bytes 1540
  170.3 8.2 %copy-start.28 = (f32[128]{0:T(128)S(1)}, f32[128]{0:T(128)}, u32[]{:S(2)}) copy-start(f32[128]{0:T(128)} %get-tuple-element.90) | copy-start | bytes 1540
  170.3 8.2 %copy-start.29 = (f32[128]{0:T(128)S(1)}, f32[128]{0:T(128)}, u32[]{:S(2)}) copy-start(f32[128]{0:T(128)} %get-tuple-element.91) | copy-start | bytes 1540
  170.4 8.2 %copy-start.30 = (f32[128]{0:T(128)S(1)}, f32[128]{0:T(128)}, u32[]{:S(2)}) copy-start(f32[128]{0:T(128)} %get-tuple-element.92) | copy-start | bytes 1540
  170.4 8.2 %copy-start.31 = (f32[128]{0:T(128)S(1)}, f32[128]{0:T(128)}, u32[]{:S(2)}) copy-start(f32[128]{0:T(128)} %get-tuple-element.93) | copy-start | bytes 1540
  170.4 8.2 %copy-start.32 = (f32[128]{0:T(128)S(1)}, f32[128]{0:T(128)}, u32[]{:S(2)}) copy-start(f32[128]{0:T(128)} %get-tuple-element.94) | copy-start | bytes 1540
  170.4 8.2 %copy-start.33 = (f32[128]{0:T(128)S(1)}, f32[128]{0:T(128)}, u32[]{:S(2)}) copy-start(f32[128]{0:T(128)} %get-tuple-element.95) | copy-start | bytes 1540
  170.4 8.2 %copy-start.34 = (f32[128]{0:T(128)S(1)}, f32[128]{0:T(128)}, u32[]{:S(2)}) copy-start(f32[128]{0:T(128)} %get-tuple-element.96) | copy-start | bytes 1540
  170.4 8.2 %copy-start.35 = (f32[128]{0:T(128)S(1)}, f32[128]{0:T(128)}, u32[]{:S(2)}) copy-start(f32[128]{0:T(128)} %get-tuple-element.97) | copy-start | bytes 1540
  170.4 8.2 %copy-start.36 = (f32[128]{0:T(128)S(1)}, f32[128]{0:T(128)}, u32[]{:S(2)}) copy-start(f32[128]{0:T(128)} %get-tuple-element.98) | copy-start | bytes 1540
  174.4 3.9 %collective-permute-start = (bf16[30,128]{1,0:T(8,128)(2,1)S(1)}, bf16[30,128]{1,0:T(8,128)(2,1)S(1)}, u32[]{:S(2)}, u32[]{:S(2)}) collective-permute-start(bf16[30,128]{1,0:T(8,128)(2,1)S(1)} %slice.265), channel_id=1, source_target_pairs={{0,32},{32,64},{64,96},{96,128},{128,160},{160,192},{192,224},{224... | collective-permute-start | bytes 23048 | tf_op jit(solution)/shard_map/ppermute | solution.py:41
  180.4 17.1 %all-to-all-start.1 = ((f32[8,1,512]{2,1,0:T(1,128)}), f32[8,1,512]{2,1,0:T(1,128)S(1)}, u32[]{:S(2)}, u32[]{:S(2)}) async-start(f32[8,1,512]{2,1,0:T(1,128)} %broadcast_in_dim.46), calls=%async_computation.1 | async-start | bytes 32768 | tf_op jit(solution)/shard_map/all_to_all | solution.py:22
Sparse Core Ops, SparseCore 0:
  20.0 102.0 all-gather.4
where the time goes:
time: 247 us; the launch traced here: 246 us
  blocking collectives  96.8 us (39%)
  waiting for transfers between devices  36.6 us (15%)
  starting transfers between devices  26.3 us (11%)
  matrix products  25.9 us (10%)
  local copies, waits for them, and re-layouts  25.3 us (10%)
  other arithmetic  20.7 us (8%)
  between operations  14.1 us (6%)
    all_to_all x1, blocking collectives, sum_at_owner(): lax.all_to_all(in_blocks(value, dim, length), axis, 0, 0, tiled=True)  30.4 us
    all_gather x1, blocking collectives, shards(): totals = lax.all_gather(device_total[None], 'sp', axis=0, tiled=True)  28.2 us
    all_gather x1, blocking collectives, shards(): piece = lax.all_gather(local_final[None], 'sp', axis=0, tiled=True)  25.9 us
    all_to_all x2, waiting for transfers between devices, from_everyone(): lax.all_to_all(jnp.broadcast_to(value[None], (length, *value.shape)), axi...  24.1 us
    all_to_all x2, starting transfers between devices, from_everyone(): lax.all_to_all(jnp.broadcast_to(value[None], (length, *value.shape)), axi...  24 us
    all_gather x1, waiting for transfers between devices, side_by_side(): lax.all_gather(both, axis, axis=dim, tiled=True)  12.5 us
    all_gather x1, blocking collectives, side_by_side(): lax.all_gather(both, axis, axis=dim, tiled=True)  12.3 us
    unnamed x76, local copies, waits for them, and re-layouts  12.3 us
  transfers between devices with their start and end apart: 4, of which 3 were waited for; matrix products, arithmetic and copies ran while one was open for 13% of the time, Pallas kernels for 0%

commit v1 on v0

--- a/solution.py
+++ b/solution.py
@@ -6,6 +6,27 @@
 DK = 32
 DV = 64
 BLOCK = 64
+
+
+def collect(shard, axis, dim):
+    size, place, rows = (lax.axis_size(axis), lax.axis_index(axis), shard.shape[dim])
+    upward = [(i, (i + 1) % size) for i in range(size)]
+    left = [(i, (i - 1) % size) for i in range(size)]
+    out = jnp.zeros((*shard.shape[:dim], size * rows, *shard.shape[dim + 1 :]), shard.dtype)
+    out = lax.dynamic_update_slice_in_dim(out, shard, place * rows, axis=dim)
+    from_left = from_right = shard
+    halfway = size // 2
+    for step in range(1, halfway + 1):
+        from_left = lax.ppermute(from_left, axis, upward)
+        out = lax.dynamic_update_slice_in_dim(
+            out, from_left, (place - step) % size * rows, axis=dim
+        )
+        if step < size - halfway:
+            from_right = lax.ppermute(from_right, axis, left)
+            out = lax.dynamic_update_slice_in_dim(
+                out, from_right, (place + step) % size * rows, axis=dim
+            )
+    return out
 
 
 def side_by_side(arrays, axis, dim, along):
@@ -195,7 +216,7 @@
     before = lax.dynamic_index_in_dim(
         running_totals, sp_index, 0, False
     ) - lax.dynamic_index_in_dim(totals, sp_index, 0, False)
-    piece = lax.all_gather(local_final[None], "sp", axis=0, tiled=True)
+    piece = collect(local_final[None], "sp", 0)
     number = piece.shape[0]
     anchor = jnp.arange(number, dtype=jnp.int32)
     exponent = jnp.where(

time: 247 us -> 272 us (1.10)
  starting transfers between devices: 26.3 us -> 66.6 us
  blocking collectives: 96.8 us -> 75.9 us
    ppermute x0 -> x15, starting transfers between devices: none -> 47.7 us  [the longest x7 29.7 us: collect(): from_right = lax.ppermute(from_right, axis, left)]
    all_gather x1 -> x0, blocking collectives: 25.9 us -> none  [shards(): piece = lax.all_gather(local_final[None], 'sp', axis=0, tiled=True)]
    all_to_all x2, starting transfers between devices: 24 us -> 17.7 us  [from_everyone(): lax.all_to_all(jnp.broadcast_to(value[None], (length, *value.shape)), axi...]
    all_to_all x1, blocking collectives: 30.4 us -> 35.4 us  [sum_at_owner(): lax.all_to_all(in_blocks(value, dim, length), axis, 0, 0, tiled=True)]
    ppermute x0 -> x15, waiting for transfers between devices: none -> 3.93 us  [the longest x8 3.91 us: collect(): from_left = lax.ppermute(from_left, axis, upward)]
    all_to_all x2, waiting for transfers between devices: 24.1 us -> 20.7 us  [from_everyone(): lax.all_to_all(jnp.broadcast_to(value[None], (length, *value.shape)), axi...]
    unnamed x76 -> x74, local copies, waits for them, and re-layouts: 12.3 us -> 13 us
  transfers between devices with their start and end apart: 4 -> 19, of which waited for: 3 -> 3; matrix products, arithmetic and copies ran while one was open for 13% -> 19% of each run, Pallas kernels for 0% -> 0%
where the time goes in v1:
time: 272 us; the launch traced here: 270 us
  blocking collectives  75.9 us (28%)
  starting transfers between devices  66.6 us (24%)
  waiting for transfers between devices  37.2 us (14%)
  matrix products  27.7 us (10%)
  local copies, waits for them, and re-layouts  27.6 us (10%)
  other arithmetic  20.7 us (8%)
  between operations  14.3 us (5%)
    all_to_all x1, blocking collectives, sum_at_owner(): lax.all_to_all(in_blocks(value, dim, length), axis, 0, 0, tiled=True)  35.4 us
    ppermute x7, starting transfers between devices, collect(): from_right = lax.ppermute(from_right, axis, left)  29.7 us
    all_gather x1, blocking collectives, shards(): totals = lax.all_gather(device_total[None], 'sp', axis=0, tiled=True)  28.2 us
    all_to_all x2, waiting for transfers between devices, from_everyone(): lax.all_to_all(jnp.broadcast_to(value[None], (length, *value.shape)), axi...  20.7 us
    ppermute x8, starting transfers between devices, collect(): from_left = lax.ppermute(from_left, axis, upward)  18 us
    all_to_all x2, starting transfers between devices, from_everyone(): lax.all_to_all(jnp.broadcast_to(value[None], (length, *value.shape)), axi...  17.7 us
    unnamed x74, local copies, waits for them, and re-layouts  13 us
    all_gather x1, waiting for transfers between devices, side_by_side(): lax.all_gather(both, axis, axis=dim, tiled=True)  12.5 us
  transfers between devices with their start and end apart: 19, of which 3 were waited for; matrix products, arithmetic and copies ran while one was open for 19% of the time, Pallas kernels for 0%

profile of v1, /device:TPU:1, one launch (start us, length us, event | category | flops | bytes accessed | tf_op | source)
XLA Modules:
  0.0 270.1 jit_solution(17423819853089002096)
XLA Ops:
  6.5 1.0 concatenate.11
  7.5 12.3 %all_gather.9 = bf16[256,896]{1,0:T(8,128)(2,1)} all-gather(bf16[64,896]{1,0:T(8,128)(2,1)S(1)} %concatenate.11), channel_id=1, replica_groups=mesh['sp'=16,'fs'=4,'tp'=8] {'fs'}, dimensions={0}, use_global_device_ids=true | all-gather | bytes 573440 | tf_op jit(solution)/shard_map/all_gather | solution.py:38
  19.8 1.1 copy.64
  20.9 1.5 broadcast_in_dim.47
  22.4 11.6 %all-to-all-start = ((bf16[8,256,512]{1,2,0:T(8,128)(2,1)}), bf16[8,256,512]{1,2,0:T(8,128)(2,1)S(1)}, u32[]{:S(2)}, u32[]{:S(2)}) async-start(bf16[8,256,512]{1,2,0:T(8,128)(2,1)} %broadcast_in_dim.47), calls=%async_computation | async-start | bytes 4194304 | tf_op jit(solution)/shard_map/all_to_all | solution.py:43
  34.0 0.8 dynamic_slice.30
  34.8 1.3 dynamic_slice.28
  36.1 1.7 dynamic-slice_bitcast_fusion.29
  37.8 1.8 fusion.100
  39.6 20.7 %all-to-all-done = bf16[8,256,512]{1,2,0:T(8,128)(2,1)S(1)} async-done(((bf16[8,256,512]{1,2,0:T(8,128)(2,1)}), bf16[8,256,512]{1,2,0:T(8,128)(2,1)S(1)}, u32[]{:S(2)}, u32[]{:S(2)}) %all-to-all-start) | async-done | bytes 2097184 | tf_op jit(solution)/shard_map/all_to_all | solution.py:43
  60.9 1.8 fusion.2
  62.6 2.2 fusion.86
  65.5 28.2 %all-gather.1 = f32[16,2,32]{2,1,0:T(2,128)S(1)} all-gather(f32[1,2,32]{2,1,0:T(2,128)S(1)} %bitcast.162), channel_id=2, replica_groups=mesh['sp'=16,'fs'=4,'tp'=8] {'sp'}, dimensions={0}, use_global_device_ids=true | all-gather | bytes 4352 | tf_op jit(solution)/shard_map/all_gather | solution.py:213
  94.0 4.5 %select_exponential_fusion = f32[4,2,64,64,32]{3,4,2,1,0:T(8,128)} fusion(f32[4,2,64,32]{2,3,1,0:T(8,128)S(1)} %copy.67, f32[4,2,64,32]{3,2,1,0:T(8,128)S(1)} %reduce_window_sum.35, pred[64,64]{1,0:T(8,128)(4,1)S(1)} %iota_compare_fusion), kind=kLoop, calls=%fused_computation.5 | loop fusion | flops 2097152 | bytes 4329472 | tf_op jit(solution)/shard_map/exp | solution.py:194
  98.5 11.0 %copy.82 = f32[4,2,64,64,32]{2,3,4,1,0:T(8,128)} copy(f32[4,2,64,64,32]{3,4,2,1,0:T(8,128)} %select_exponential_fusion) | data formatting | bytes 8388608
  109.5 12.5 %all-gather.4.cloned.1.call-done = bf16[4096,896]{1,0:T(8,128)(2,1)} async-done(((bf16[256,896]{1,0:T(8,128)(2,1)}), bf16[4096,896]{1,0:T(8,128)(2,1)}) %all-gather.4.cloned.1.call-update) | async-done | bytes 7340048 | tf_op jit(solution)/shard_map/all_gather | solution.py:38
  122.1 2.2 fusion.18
  124.4 0.8 copy.73
  125.3 2.0 fusion.13
  127.4 2.0 fusion.38
  129.3 5.8 %while.13 = (s32[]{:T(128)}, f32[2,32,64]{2,1,0:T(8,128)S(1)}, f32[4,2,32,64]{3,2,1,0:T(8,128)}, f32[4,2,32]{2,1,0:T(2,128)S(1)}, f32[4,2,32,64]{3,2,1,0:T(8,128)}, /*index=5*/s32[]{:T(128)}, s32[]{:T(128)}) while((s32[]{:T(128)}, f32[2,32,64]{2,1,0:T(8,128)S(1)}, f32[4,2,32,64]{3,2,1,0:T(8,128)}, f32[4,2,32]{2,1,0:T(2,128)S(1)}, ...), condition=%wide.region_9.10_spmd.clone, body=%wide.region_8.9_spmd.clone.sunk | while | flops 16387 | bytes 99680 | solution.py:209
  130.0 0.8 bitcast_add_fusion.3
  130.8 0.6 bitcast_dynamic-update-slice_fusion.2
  131.4 0.8 bitcast_add_fusion.3
  132.2 0.6 bitcast_dynamic-update-slice_fusion.2
  132.9 0.8 bitcast_add_fusion.3
  133.7 0.6 bitcast_dynamic-update-slice_fusion.2
  134.3 0.8 bitcast_add_fusion.3
  135.2 1.9 collective-permute-start.1
  137.1 4.6 %collective-permute-start.2 = (f32[1,2,32,64]{3,2,1,0:T(8,128)S(1)}, f32[1,2,32,64]{3,2,1,0:T(8,128)}, u32[]{:S(2)}, u32[]{:S(2)}) collective-permute-start(f32[1,2,32,64]{3,2,1,0:T(8,128)S(1)} %bitcast.153), channel_id=1, source_target_pairs={{0,480},{32,0},{64,32},{96,64},{128,96},{160,128},{192,160},{224,1... | collective-permute-start | bytes 49160 | tf_op jit(solution)/shard_map/ppermute | solution.py:25
  141.7 0.7 copy.68
  142.3 1.8 fusion.21
  144.2 5.3 %fusion = f32[4,2,64,64]{2,3,1,0:T(8,128)S(1)} fusion(f32[4,2,64,64,32]{2,3,4,1,0:T(8,128)} %copy.82, f32[4,2,32,64]{3,2,1,0:T(8,128)S(1)} %copy.69, f32[4,2,32,64]{3,2,1,0:T(8,128)} %copy.68), kind=kLoop, calls=%fused_computation.4 | loop fusion | flops 3112960 | bytes 4456448 | tf_op jit(solution)/shard_map/nhid,nhjd,nhijd->nhij/dot_general | solution.py:195
  149.5 1.0 fusion.73
  150.8 2.0 fusion.12
  152.8 2.0 fusion.6
  154.8 1.3 collective-permute-start
  156.1 0.9 copy.72
  157.3 1.8 fusion.103
  159.1 0.6 broadcast_in_dim.48
  159.7 6.1 %all-to-all-start.1 = ((f32[8,1,512]{2,1,0:T(1,128)}), f32[8,1,512]{2,1,0:T(1,128)S(1)}, u32[]{:S(2)}, u32[]{:S(2)}) async-start(f32[8,1,512]{2,1,0:T(1,128)} %broadcast_in_dim.48), calls=%async_computation.1 | async-start | bytes 32768 | tf_op jit(solution)/shard_map/all_to_all | solution.py:43
  165.8 3.9 %collective-permute-start.3 = (f32[1,2,32,64]{3,2,1,0:T(8,128)}, f32[1,2,32,64]{3,2,1,0:T(8,128)S(1)}, u32[]{:S(2)}, u32[]{:S(2)}) collective-permute-start(f32[1,2,32,64]{3,2,1,0:T(8,128)} %collective-permute-done.1), channel_id=1, source_target_pairs={{0,32},{32,64},{64,96},{96,128},{128,160},{160,192},{192,224},{224... | collective-permute-start | bytes 49160 | tf_op jit(solution)/shard_map/ppermute | solution.py:20
  169.7 2.9 %collective-permute-start.4 = (f32[1,2,32,64]{3,2,1,0:T(8,128)}, f32[1,2,32,64]{3,2,1,0:T(8,128)S(1)}, u32[]{:S(2)}, u32[]{:S(2)}) collective-permute-start(f32[1,2,32,64]{3,2,1,0:T(8,128)} %collective-permute-done.2), channel_id=1, source_target_pairs={{0,480},{32,0},{64,32},{96,64},{128,96},{160,128},{192,160},{224,1... | collective-permute-start | bytes 49160 | tf_op jit(solution)/shard_map/ppermute | solution.py:25
  172.6 0.8 constant_dynamic-update-slice_fusion.14
  173.4 0.8 constant_dynamic-update-slice_fusion.13
  174.2 0.8 copy-done.3
  174.9 4.2 %fusion.31 = f32[4096,256]{1,0:T(8,128)} fusion(bf16[4096,896]{1,0:T(8,128)(2,1)} %all-gather.4.cloned.1.call-done, f32[256,128]{1,0:T(8,128)} %get-tuple-element.65, f32[128]{0:T(128)} %dynamic_slice.28, f32[256]{0:T(256)S(1)} %get-tuple-element.100, f32[256]{0:T(256)S(1)} %get-tuple-element.99), kind=kOutput, calls=%fused_computation.50 | convolution fusion | flops 268697600 | bytes 5376512 | tf_op jit(solution)/shard_map/dot_general | solution.py:243
  179.2 2.6 collective-permute-start.5
  181.8 3.9 %collective-permute-start.6 = (f32[1,2,32,64]{3,2,1,0:T(8,128)S(1)}, f32[1,2,32,64]{3,2,1,0:T(8,128)S(1)}, u32[]{:S(2)}, u32[]{:S(2)}) collective-permute-start(f32[1,2,32,64]{3,2,1,0:T(8,128)S(1)} %collective-permute-done.4), channel_id=1, source_target_pairs={{0,480},{32,0},{64,32},{96,64},{128,96},{160,128},{192,160},{224,1... | collective-permute-start | bytes 49160 | tf_op jit(solution)/shard_map/ppermute | solution.py:25
  185.7 1.9 collective-permute-start.7
  187.7 4.6 %collective-permute-start.8 = (f32[1,2,32,64]{3,2,1,0:T(8,128)S(1)}, f32[1,2,32,64]{3,2,1,0:T(8,128)S(1)}, u32[]{:S(2)}, u32[]{:S(2)}) collective-permute-start(f32[1,2,32,64]{3,2,1,0:T(8,128)S(1)} %collective-permute-done.6), channel_id=1, source_target_pairs={{0,480},{32,0},{64,32},{96,64},{128,96},{160,128},{192,160},{224,1... | collective-permute-start | bytes 49160 | tf_op jit(solution)/shard_map/ppermute | solution.py:25
  192.3 1.9 collective-permute-start.9
  194.2 4.6 %collective-permute-start.10 = (f32[1,2,32,64]{3,2,1,0:T(8,128)S(1)}, f32[1,2,32,64]{3,2,1,0:T(8,128)S(1)}, u32[]{:S(2)}, u32[]{:S(2)}) collective-permute-start(f32[1,2,32,64]{3,2,1,0:T(8,128)S(1)} %collective-permute-done.8), channel_id=1, source_target_pairs={{0,480},{32,0},{64,32},{96,64},{128,96},{160,128},{192,160},{224,1... | collective-permute-start | bytes 49160 | tf_op jit(solution)/shard_map/ppermute | solution.py:25
  198.9 1.9 collective-permute-start.11
  200.8 4.6 %collective-permute-start.12 = (f32[1,2,32,64]{3,2,1,0:T(8,128)S(1)}, f32[1,2,32,64]{3,2,1,0:T(8,128)S(1)}, u32[]{:S(2)}, u32[]{:S(2)}) collective-permute-start(f32[1,2,32,64]{3,2,1,0:T(8,128)S(1)} %collective-permute-done.10), channel_id=1, source_target_pairs={{0,480},{32,0},{64,32},{96,64},{128,96},{160,128},{192,160},{224,1... | collective-permute-start | bytes 49160 | tf_op jit(solution)/shard_map/ppermute | solution.py:25
  205.4 1.9 collective-permute-start.13
  207.4 4.6 %collective-permute-start.14 = (f32[1,2,32,64]{3,2,1,0:T(8,128)S(1)}, f32[1,2,32,64]{3,2,1,0:T(8,128)S(1)}, u32[]{:S(2)}, u32[]{:S(2)}) collective-permute-start(f32[1,2,32,64]{3,2,1,0:T(8,128)S(1)} %collective-permute-done.12), channel_id=1, source_target_pairs={{0,480},{32,0},{64,32},{96,64},{128,96},{160,128},{192,160},{224,1... | collective-permute-start | bytes 49160 | tf_op jit(solution)/shard_map/ppermute | solution.py:25
  212.0 1.9 collective-permute-start.15
  214.0 3.9 %collective-permute-done.15 = f32[1,2,32,64]{3,2,1,0:T(8,128)S(1)} collective-permute-done((f32[1,2,32,64]{3,2,1,0:T(8,128)S(1)}, f32[1,2,32,64]{3,2,1,0:T(8,128)S(1)}, u32[]{:S(2)}, u32[]{:S(2)}) %collective-permute-start.15) | collective-permute-done | bytes 16416 | tf_op jit(solution)/shard_map/ppermute | solution.py:20
  217.9 0.9 fusion.34
  218.8 1.7 multiply_reduce_fusion.1
  221.0 5.7 %fusion.1 = bf16[4096,256]{1,0:T(8,128)(2,1)} fusion(f32[4096,256]{1,0:T(8,128)} %fusion.31, bf16[4096,896]{1,0:T(8,128)(2,1)} %all-gather.4.cloned.1.call-done, f32[256,128]{1,0:T(8,128)S(1)} %reshape.78, bf16[256,4096]{0,1:T(8,128)(2,1)S(1)} %copy-done.2, f32[256]{0:T(256)S(1)} %add_rsqrt_fusion.1), kind=kOutput, calls=%fused_computation.7 | convolution fusion | flops 539262976 | bytes 10617856 | tf_op jit(solution)/shard_map/dot_general | solution.py:249
  226.7 35.4 %all_to_all.16 = bf16[8,512,256]{2,1,0:T(8,128)(2,1)S(1)} all-to-all(bf16[8,512,256]{2,1,0:T(8,128)(2,1)} %bitcast.151), channel_id=1, replica_groups=mesh['sp'=16,'fs'=4,'tp'=8] {'tp'}, dimensions={0} | all-to-all | bytes 4194304 | tf_op jit(solution)/shard_map/all_to_all | solution.py:87
  262.4 0.8 copy.77
  (140 shorter events, 3.7 us)
Async XLA Ops:
  6.5 56.1 %copy-start = (bf16[4096,64]{0,1:T(8,128)(2,1)S(1)}, bf16[4096,64]{0,1:T(8,128)(2,1)}, u32[]{:S(2)}) copy-start(bf16[4096,64]{0,1:T(8,128)(2,1)} %param.29) | copy-start | bytes 1572868
  6.5 115.5 %all-gather.4.cloned.1.call-start = ((), (), s32[]{:S(2)}) async-start(), calls=%async_computation.3 | async-start | bytes 7798784 | tf_op jit(solution)/shard_map/all_gather | solution.py:38
  20.9 39.9 %copy-start.7 = (f32[4096]{0:T(1024)S(1)}, f32[4096]{0:T(1024)}, u32[]{:S(2)}) copy-start(f32[4096]{0:T(1024)} %param.20) | copy-start | bytes 49156
  22.4 37.8 %all-to-all-start = ((bf16[8,256,512]{1,2,0:T(8,128)(2,1)}), bf16[8,256,512]{1,2,0:T(8,128)(2,1)S(1)}, u32[]{:S(2)}, u32[]{:S(2)}) async-start(bf16[8,256,512]{1,2,0:T(8,128)(2,1)} %broadcast_in_dim.47), calls=%async_computation | async-start | bytes 4194304 | tf_op jit(solution)/shard_map/all_to_all | solution.py:43
  34.0 28.6 %copy-start.6 = (f32[1,256,64]{1,2,0:T(8,128)S(1)}, f32[1,256,64]{1,2,0:T(8,128)}, u32[]{:S(2)}) copy-start(f32[1,256,64]{1,2,0:T(8,128)} %param.32) | copy-start | bytes 196612
  98.5 23.6 %copy-start.1 = (bf16[256,4096]{0,1:T(8,128)(2,1)S(1)}, bf16[256,4096]{0,1:T(8,128)(2,1)}, u32[]{:S(2)}) copy-start(bf16[256,4096]{0,1:T(8,128)(2,1)} %fusion.2) | copy-start | bytes 6291460
  135.2 30.6 %collective-permute-start.1 = (f32[1,2,32,64]{3,2,1,0:T(8,128)S(1)}, f32[1,2,32,64]{3,2,1,0:T(8,128)}, u32[]{:S(2)}, u32[]{:S(2)}) collective-permute-start(f32[1,2,32,64]{3,2,1,0:T(8,128)S(1)} %bitcast.152), channel_id=1, source_target_pairs={{0,32},{32,64},{64,96},{96,128},{128,160},{160,192},{192,224},{224... | collective-permute-start | bytes 49160 | tf_op jit(solution)/shard_map/ppermute | solution.py:20
  137.1 32.6 %collective-permute-start.2 = (f32[1,2,32,64]{3,2,1,0:T(8,128)S(1)}, f32[1,2,32,64]{3,2,1,0:T(8,128)}, u32[]{:S(2)}, u32[]{:S(2)}) collective-permute-start(f32[1,2,32,64]{3,2,1,0:T(8,128)S(1)} %bitcast.153), channel_id=1, source_target_pairs={{0,480},{32,0},{64,32},{96,64},{128,96},{160,128},{192,160},{224,1... | collective-permute-start | bytes 49160 | tf_op jit(solution)/shard_map/ppermute | solution.py:25
  150.5 6.5 %copy-start.8 = (f32[128]{0:T(128)S(1)}, f32[128]{0:T(128)}, u32[]{:S(2)}) copy-start(f32[128]{0:T(128)} %get-tuple-element.69) | copy-start | bytes 1540
  150.5 6.5 %copy-start.9 = (f32[128]{0:T(128)S(1)}, f32[128]{0:T(128)}, u32[]{:S(2)}) copy-start(f32[128]{0:T(128)} %get-tuple-element.70) | copy-start | bytes 1540
  150.5 6.5 %copy-start.10 = (f32[128]{0:T(128)S(1)}, f32[128]{0:T(128)}, u32[]{:S(2)}) copy-start(f32[128]{0:T(128)} %get-tuple-element.71) | copy-start | bytes 1540
  150.5 6.5 %copy-start.11 = (f32[128]{0:T(128)S(1)}, f32[128]{0:T(128)}, u32[]{:S(2)}) copy-start(f32[128]{0:T(128)} %get-tuple-element.72) | copy-start | bytes 1540
  150.5 6.5 %copy-start.12 = (f32[128]{0:T(128)S(1)}, f32[128]{0:T(128)}, u32[]{:S(2)}) copy-start(f32[128]{0:T(128)} %get-tuple-element.73) | copy-start | bytes 1540
  150.6 6.5 %copy-start.13 = (f32[128]{0:T(128)S(1)}, f32[128]{0:T(128)}, u32[]{:S(2)}) copy-start(f32[128]{0:T(128)} %get-tuple-element.74) | copy-start | bytes 1540
  150.6 6.5 %copy-start.14 = (f32[128]{0:T(128)S(1)}, f32[128]{0:T(128)}, u32[]{:S(2)}) copy-start(f32[128]{0:T(128)} %get-tuple-element.75) | copy-start | bytes 1540
  150.6 6.5 %copy-start.15 = (f32[128]{0:T(128)S(1)}, f32[128]{0:T(128)}, u32[]{:S(2)}) copy-start(f32[128]{0:T(128)} %get-tuple-element.76) | copy-start | bytes 1540
  150.6 6.5 %copy-start.16 = (f32[128]{0:T(128)S(1)}, f32[128]{0:T(128)}, u32[]{:S(2)}) copy-start(f32[128]{0:T(128)} %get-tuple-element.77) | copy-start | bytes 1540
  150.6 6.5 %copy-start.17 = (f32[128]{0:T(128)S(1)}, f32[128]{0:T(128)}, u32[]{:S(2)}) copy-start(f32[128]{0:T(128)} %get-tuple-element.78) | copy-start | bytes 1540
  150.6 6.5 %copy-start.18 = (f32[128]{0:T(128)S(1)}, f32[128]{0:T(128)}, u32[]{:S(2)}) copy-start(f32[128]{0:T(128)} %get-tuple-element.79) | copy-start | bytes 1540
  150.6 6.5 %copy-start.19 = (f32[128]{0:T(128)S(1)}, f32[128]{0:T(128)}, u32[]{:S(2)}) copy-start(f32[128]{0:T(128)} %get-tuple-element.80) | copy-start | bytes 1540
  150.6 6.5 %copy-start.20 = (f32[128]{0:T(128)S(1)}, f32[128]{0:T(128)}, u32[]{:S(2)}) copy-start(f32[128]{0:T(128)} %get-tuple-element.81) | copy-start | bytes 1540
  150.6 6.5 %copy-start.21 = (f32[128]{0:T(128)S(1)}, f32[128]{0:T(128)}, u32[]{:S(2)}) copy-start(f32[128]{0:T(128)} %get-tuple-element.82) | copy-start | bytes 1540
  150.6 6.5 %copy-start.22 = (f32[128]{0:T(128)S(1)}, f32[128]{0:T(128)}, u32[]{:S(2)}) copy-start(f32[128]{0:T(128)} %get-tuple-element.83) | copy-start | bytes 1540
  150.7 6.5 %copy-start.23 = (f32[128]{0:T(128)S(1)}, f32[128]{0:T(128)}, u32[]{:S(2)}) copy-start(f32[128]{0:T(128)} %get-tuple-element.84) | copy-start | bytes 1540
  150.7 6.5 %copy-start.24 = (f32[128]{0:T(128)S(1)}, f32[128]{0:T(128)}, u32[]{:S(2)}) copy-start(f32[128]{0:T(128)} %get-tuple-element.85) | copy-start | bytes 1540
  150.7 6.5 %copy-start.25 = (f32[128]{0:T(128)S(1)}, f32[128]{0:T(128)}, u32[]{:S(2)}) copy-start(f32[128]{0:T(128)} %get-tuple-element.86) | copy-start | bytes 1540
  150.7 6.5 %copy-start.26 = (f32[128]{0:T(128)S(1)}, f32[128]{0:T(128)}, u32[]{:S(2)}) copy-start(f32[128]{0:T(128)} %get-tuple-element.87) | copy-start | bytes 1540
  150.7 6.5 %copy-start.27 = (f32[128]{0:T(128)S(1)}, f32[128]{0:T(128)}, u32[]{:S(2)}) copy-start(f32[128]{0:T(128)} %get-tuple-element.88) | copy-start | bytes 1540
  150.7 6.5 %copy-start.28 = (f32[128]{0:T(128)S(1)}, f32[128]{0:T(128)}, u32[]{:S(2)}) copy-start(f32[128]{0:T(128)} %get-tuple-element.89) | copy-start | bytes 1540
  150.7 6.5 %copy-start.29 = (f32[128]{0:T(128)S(1)}, f32[128]{0:T(128)}, u32[]{:S(2)}) copy-start(f32[128]{0:T(128)} %get-tuple-element.90) | copy-start | bytes 1540
  150.7 6.5 %copy-start.30 = (f32[128]{0:T(128)S(1)}, f32[128]{0:T(128)}, u32[]{:S(2)}) copy-start(f32[128]{0:T(128)} %get-tuple-element.91) | copy-start | bytes 1540
  150.7 6.5 %copy-start.31 = (f32[128]{0:T(128)S(1)}, f32[128]{0:T(128)}, u32[]{:S(2)}) copy-start(f32[128]{0:T(128)} %get-tuple-element.92) | copy-start | bytes 1540
  150.7 6.5 %copy-start.32 = (f32[128]{0:T(128)S(1)}, f32[128]{0:T(128)}, u32[]{:S(2)}) copy-start(f32[128]{0:T(128)} %get-tuple-element.93) | copy-start | bytes 1540
  150.8 6.5 %copy-start.33 = (f32[128]{0:T(128)S(1)}, f32[128]{0:T(128)}, u32[]{:S(2)}) copy-start(f32[128]{0:T(128)} %get-tuple-element.94) | copy-start | bytes 1540
  150.8 6.5 %copy-start.34 = (f32[128]{0:T(128)S(1)}, f32[128]{0:T(128)}, u32[]{:S(2)}) copy-start(f32[128]{0:T(128)} %get-tuple-element.95) | copy-start | bytes 1540
  154.8 2.2 collective-permute-start
  159.1 59.6 %copy-start.5 = (f32[4,2,64,64]{2,3,1,0:T(8,128)S(1)}, f32[4,2,64,64]{2,3,1,0:T(8,128)}, u32[]{:S(2)}) copy-start(f32[4,2,64,64]{2,3,1,0:T(8,128)} %fusion.73) | copy-start | bytes 393220
  159.1 61.4 %copy-start.35 = (f32[64]{0:T(128)S(1)}, f32[64]{0:T(128)}, u32[]{:S(2)}) copy-start(f32[64]{0:T(128)} %param.35) | copy-start | bytes 772
  159.7 14.4 %all-to-all-start.1 = ((f32[8,1,512]{2,1,0:T(1,128)}), f32[8,1,512]{2,1,0:T(1,128)S(1)}, u32[]{:S(2)}, u32[]{:S(2)}) async-start(f32[8,1,512]{2,1,0:T(1,128)} %broadcast_in_dim.48), calls=%async_computation.1 | async-start | bytes 32768 | tf_op jit(solution)/shard_map/all_to_all | solution.py:43
  165.8 13.4 %collective-permute-start.3 = (f32[1,2,32,64]{3,2,1,0:T(8,128)}, f32[1,2,32,64]{3,2,1,0:T(8,128)S(1)}, u32[]{:S(2)}, u32[]{:S(2)}) collective-permute-start(f32[1,2,32,64]{3,2,1,0:T(8,128)} %collective-permute-done.1), channel_id=1, source_target_pairs={{0,32},{32,64},{64,96},{96,128},{128,160},{160,192},{192,224},{224... | collective-permute-start | bytes 49160 | tf_op jit(solution)/shard_map/ppermute | solution.py:20
  169.7 12.0 %collective-permute-start.4 = (f32[1,2,32,64]{3,2,1,0:T(8,128)}, f32[1,2,32,64]{3,2,1,0:T(8,128)S(1)}, u32[]{:S(2)}, u32[]{:S(2)}) collective-permute-start(f32[1,2,32,64]{3,2,1,0:T(8,128)} %collective-permute-done.2), channel_id=1, source_target_pairs={{0,480},{32,0},{64,32},{96,64},{128,96},{160,128},{192,160},{224,1... | collective-permute-start | bytes 49160 | tf_op jit(solution)/shard_map/ppermute | solution.py:25
  174.1 0.8 copy-start.3
  174.9 10.7 %copy-start.4 = (f32[16,2,32,64]{3,2,1,0:T(8,128)S(1)}, f32[16,2,32,64]{3,2,1,0:T(8,128)}, u32[]{:S(2)}) copy-start(f32[16,2,32,64]{3,2,1,0:T(8,128)} %copy-done.3) | copy-start | bytes 786436
  174.9 46.0 %copy-start.2 = (bf16[256,4096]{0,1:T(8,128)(2,1)S(1)}, bf16[256,4096]{0,1:T(8,128)(2,1)}, u32[]{:S(2)}) copy-start(bf16[256,4096]{0,1:T(8,128)(2,1)} %fusion.2) | copy-start | bytes 6291460
  179.2 6.6 %collective-permute-start.5 = (f32[1,2,32,64]{3,2,1,0:T(8,128)S(1)}, f32[1,2,32,64]{3,2,1,0:T(8,128)S(1)}, u32[]{:S(2)}, u32[]{:S(2)}) collective-permute-start(f32[1,2,32,64]{3,2,1,0:T(8,128)S(1)} %collective-permute-done.3), channel_id=1, source_target_pairs={{0,32},{32,64},{64,96},{96,128},{128,160},{160,192},{192,224},{224... | collective-permute-start | bytes 49160 | tf_op jit(solution)/shard_map/ppermute | solution.py:20
  181.8 5.9 %collective-permute-start.6 = (f32[1,2,32,64]{3,2,1,0:T(8,128)S(1)}, f32[1,2,32,64]{3,2,1,0:T(8,128)S(1)}, u32[]{:S(2)}, u32[]{:S(2)}) collective-permute-start(f32[1,2,32,64]{3,2,1,0:T(8,128)S(1)} %collective-permute-done.4), channel_id=1, source_target_pairs={{0,480},{32,0},{64,32},{96,64},{128,96},{160,128},{192,160},{224,1... | collective-permute-start | bytes 49160 | tf_op jit(solution)/shard_map/ppermute | solution.py:25
  185.7 6.6 %collective-permute-start.7 = (f32[1,2,32,64]{3,2,1,0:T(8,128)S(1)}, f32[1,2,32,64]{3,2,1,0:T(8,128)S(1)}, u32[]{:S(2)}, u32[]{:S(2)}) collective-permute-start(f32[1,2,32,64]{3,2,1,0:T(8,128)S(1)} %collective-permute-done.5), channel_id=1, source_target_pairs={{0,32},{32,64},{64,96},{96,128},{128,160},{160,192},{192,224},{224... | collective-permute-start | bytes 49160 | tf_op jit(solution)/shard_map/ppermute | solution.py:20
  187.7 6.6 %collective-permute-start.8 = (f32[1,2,32,64]{3,2,1,0:T(8,128)S(1)}, f32[1,2,32,64]{3,2,1,0:T(8,128)S(1)}, u32[]{:S(2)}, u32[]{:S(2)}) collective-permute-start(f32[1,2,32,64]{3,2,1,0:T(8,128)S(1)} %collective-permute-done.6), channel_id=1, source_target_pairs={{0,480},{32,0},{64,32},{96,64},{128,96},{160,128},{192,160},{224,1... | collective-permute-start | bytes 49160 | tf_op jit(solution)/shard_map/ppermute | solution.py:25
  192.3 6.6 %collective-permute-start.9 = (f32[1,2,32,64]{3,2,1,0:T(8,128)S(1)}, f32[1,2,32,64]{3,2,1,0:T(8,128)S(1)}, u32[]{:S(2)}, u32[]{:S(2)}) collective-permute-start(f32[1,2,32,64]{3,2,1,0:T(8,128)S(1)} %collective-permute-done.7), channel_id=1, source_target_pairs={{0,32},{32,64},{64,96},{96,128},{128,160},{160,192},{192,224},{224... | collective-permute-start | bytes 49160 | tf_op jit(solution)/shard_map/ppermute | solution.py:20
  194.2 6.6 %collective-permute-start.10 = (f32[1,2,32,64]{3,2,1,0:T(8,128)S(1)}, f32[1,2,32,64]{3,2,1,0:T(8,128)S(1)}, u32[]{:S(2)}, u32[]{:S(2)}) collective-permute-start(f32[1,2,32,64]{3,2,1,0:T(8,128)S(1)} %collective-permute-done.8), channel_id=1, source_target_pairs={{0,480},{32,0},{64,32},{96,64},{128,96},{160,128},{192,160},{224,1... | collective-permute-start | bytes 49160 | tf_op jit(solution)/shard_map/ppermute | solution.py:25
  198.9 6.6 %collective-permute-start.11 = (f32[1,2,32,64]{3,2,1,0:T(8,128)S(1)}, f32[1,2,32,64]{3,2,1,0:T(8,128)S(1)}, u32[]{:S(2)}, u32[]{:S(2)}) collective-permute-start(f32[1,2,32,64]{3,2,1,0:T(8,128)S(1)} %collective-permute-done.9), channel_id=1, source_target_pairs={{0,32},{32,64},{64,96},{96,128},{128,160},{160,192},{192,224},{224... | collective-permute-start | bytes 49160 | tf_op jit(solution)/shard_map/ppermute | solution.py:20
  200.8 6.6 %collective-permute-start.12 = (f32[1,2,32,64]{3,2,1,0:T(8,128)S(1)}, f32[1,2,32,64]{3,2,1,0:T(8,128)S(1)}, u32[]{:S(2)}, u32[]{:S(2)}) collective-permute-start(f32[1,2,32,64]{3,2,1,0:T(8,128)S(1)} %collective-permute-done.10), channel_id=1, source_target_pairs={{0,480},{32,0},{64,32},{96,64},{128,96},{160,128},{192,160},{224,1... | collective-permute-start | bytes 49160 | tf_op jit(solution)/shard_map/ppermute | solution.py:25
  205.4 6.6 %collective-permute-start.13 = (f32[1,2,32,64]{3,2,1,0:T(8,128)S(1)}, f32[1,2,32,64]{3,2,1,0:T(8,128)S(1)}, u32[]{:S(2)}, u32[]{:S(2)}) collective-permute-start(f32[1,2,32,64]{3,2,1,0:T(8,128)S(1)} %collective-permute-done.11), channel_id=1, source_target_pairs={{0,32},{32,64},{64,96},{96,128},{128,160},{160,192},{192,224},{224... | collective-permute-start | bytes 49160 | tf_op jit(solution)/shard_map/ppermute | solution.py:20
  207.4 6.6 %collective-permute-start.14 = (f32[1,2,32,64]{3,2,1,0:T(8,128)S(1)}, f32[1,2,32,64]{3,2,1,0:T(8,128)S(1)}, u32[]{:S(2)}, u32[]{:S(2)}) collective-permute-start(f32[1,2,32,64]{3,2,1,0:T(8,128)S(1)} %collective-permute-done.12), channel_id=1, source_target_pairs={{0,480},{32,0},{64,32},{96,64},{128,96},{160,128},{192,160},{224,1... | collective-permute-start | bytes 49160 | tf_op jit(solution)/shard_map/ppermute | solution.py:25
  212.0 5.9 %collective-permute-start.15 = (f32[1,2,32,64]{3,2,1,0:T(8,128)S(1)}, f32[1,2,32,64]{3,2,1,0:T(8,128)S(1)}, u32[]{:S(2)}, u32[]{:S(2)}) collective-permute-start(f32[1,2,32,64]{3,2,1,0:T(8,128)S(1)} %collective-permute-done.13), channel_id=1, source_target_pairs={{0,32},{32,64},{64,96},{96,128},{128,160},{160,192},{192,224},{224... | collective-permute-start | bytes 49160 | tf_op jit(solution)/shard_map/ppermute | solution.py:20
Sparse Core Ops, SparseCore 0:
  20.0 102.0 all-gather.3
